TPU v7x, 32 devices: a whole 2x2x4 slice. The times are simulated.
32 devices in a mesh: kv: 8 (over z, x), tp: 4 (over y, core).
Axes of the slice: x: 2, y: 2, z: 4, core: 2. Of those that a mesh axis runs over, the one named last changes fastest.
Arguments:
- hidden: bfloat16 [512, 4096], P(None, 'kv'), as said below
- norm_gain: bfloat16 [4096], replicated, may hold values from 0.099609375 to 1.8984375
- w_query: bfloat16 [4096, 4096], P('kv', 'tp'), may hold values from -0.09375 to 0.09375
- w_key: bfloat16 [4096, 4096], P('kv', 'tp'), may hold values from -0.09375 to 0.09375
- w_value: bfloat16 [4096, 8192], P('kv', 'tp'), may hold values from -0.09375 to 0.09375
- w_gate: bfloat16 [4096, 8192], P('kv', 'tp'), may hold values from -0.09375 to 0.09375
- w_write: bfloat16 [4096, 32], P('kv', 'tp'), may hold values from -0.09375 to 0.09375
- w_decay: bfloat16 [4096, 32], P('kv', 'tp'), may hold values from -0.09375 to 0.09375
- w_out: bfloat16 [8192, 4096], P('tp', 'kv'), may hold values from -0.0625 to 0.0625
- decay_rate: float32 [32], P('tp'), may hold values from 0 to 4, as said below
- head_gain: float32 [256], replicated, may hold values from 0.1 to 1.9
- carried_state: float32 [128, 32, 128, 256], P('kv', 'tp'), may hold values from -4 to 4
- last_keys: bfloat16 [128, 4, 4096], P('kv', None, 'tp'), may hold values from -6 to 6
- last_values: bfloat16 [128, 4, 8192], P('kv', None, 'tp'), may hold values from -6 to 6
- last_writes: float32 [128, 4, 32], P('kv', None, 'tp'), may hold values from -6 to 6
- last_decays: float32 [128, 4, 32], P('kv', None, 'tp'), may hold values from -6 to 6
- accepted: int32 [128], P('kv'), may hold values from 0 to 4
Outputs:
- mixed_out: bfloat16 [512, 4096], P('tp', 'kv')
- committed: float32 [128, 32, 128, 256], P('kv', 'tp')
Inputs may be any that keep to these rules, and one draw needn't show every extreme that they name: `decay_rate`: positive. `hidden`: finite real values.
All inputs are finite; a program needn't handle non-finite values.
Results may differ from a plain program's by a relative error of at most 0.029.
Values may be sent and summed in bfloat16 or wider, within the bound.
A program may use at most 128 MiB of HBM per device.

v0:
```python
import jax
import jax.numpy as jnp
from jax import lax
from jax.sharding import PartitionSpec as P

D = 4096


norm_eps = 1e-06
highest = lax.Precision.HIGHEST


def unit_rows(matrix):
    return matrix * lax.rsqrt(jnp.sum(matrix * matrix, -1, keepdims=True) + norm_eps)


def corrected(key_rows, values, write_rate, log_decay, start_state):
    proposals = key_rows.shape[2]
    value_width = values.shape[-1]
    running = jnp.cumsum(log_decay, axis=-1)
    causal = jnp.tril(jnp.ones((proposals, proposals), dtype=bool))
    spread = running[..., :, None] - running[..., None, :]
    weights = jnp.where(causal, jnp.exp(jnp.where(causal, spread, 0.0)), 0.0)
    strong_keys = key_rows * write_rate[..., None]
    lower_part = jnp.einsum("bhcd,bhsd->bhcs", strong_keys, key_rows, precision=highest)
    lower_part = lower_part * weights * (1.0 - jnp.eye(proposals, dtype=jnp.float32))
    right_side = jnp.concatenate(
        [values * write_rate[..., None], strong_keys * jnp.exp(running)[..., None]], -1
    )
    solved_rows = []
    for later in range(proposals):
        current = right_side[..., later, :]
        for early in range(later):
            current = current - lower_part[..., later, early, None] * solved_rows[early]
        solved_rows.append(current)
    solved = jnp.stack(solved_rows, axis=2)
    fresh_values = solved[..., :value_width] - jnp.einsum(
        "bhcd,bhde->bhce", solved[..., value_width:], start_state, precision=highest
    )
    return (fresh_values, running, weights)


def advance(key_rows, fresh_values, running, start_state):
    tail_decay = jnp.exp(running[..., -1:] - running)
    return start_state * jnp.exp(running[..., -1])[..., None, None] + jnp.einsum(
        "bhcd,bhce->bhde", key_rows * tail_decay[..., None], fresh_values, precision=highest
    )


def readout(queries, key_rows, fresh_values, running, weights, start_state):
    scores = jnp.einsum("bhcd,bhsd->bhcs", queries, key_rows, precision=highest) * weights
    carried = jnp.einsum(
        "bhcd,bhde->bhce", queries * jnp.exp(running)[..., None], start_state, precision=highest
    )
    return carried + jnp.einsum("bhcs,bhse->bhce", scores, fresh_values, precision=highest)


def core(
    proj_query,
    proj_key,
    proj_value,
    proj_gate,
    proj_write,
    proj_decay,
    decay_rate,
    head_gain,
    carried_state,
    last_keys,
    last_values,
    last_writes,
    last_decays,
    accepted,
):
    seq_count, head_count, key_width, value_width = carried_state.shape
    proposals = last_keys.shape[1]

    def by_head(matrix, width):
        return jnp.transpose(matrix.reshape(seq_count, proposals, head_count, width), (0, 2, 1, 3))

    def by_head_small(matrix):
        return jnp.transpose(matrix.reshape(seq_count, proposals, head_count), (0, 2, 1))

    rates = decay_rate[None, :, None]
    taken = (jnp.arange(proposals, dtype=jnp.int32)[None, :] < accepted[:, None]).astype(
        jnp.float32
    )[:, None, :]
    old_keys = unit_rows(by_head(last_keys.astype(jnp.float32), key_width))
    old_values = by_head(last_values.astype(jnp.float32), value_width)
    old_write = jax.nn.sigmoid(by_head_small(last_writes)) * taken
    old_decay = -rates * jax.nn.softplus(by_head_small(last_decays)) * taken
    fresh_values, running, weights = corrected(
        old_keys, old_values, old_write, old_decay, carried_state
    )
    committed = advance(old_keys, fresh_values, running, carried_state)
    queries = unit_rows(by_head(jax.nn.silu(proj_query), key_width)) * key_width ** (-0.5)
    key_rows = unit_rows(by_head(jax.nn.silu(proj_key), key_width))
    values = by_head(jax.nn.silu(proj_value), value_width)
    write_rate = jax.nn.sigmoid(by_head_small(proj_write))
    log_decay = -rates * jax.nn.softplus(by_head_small(proj_decay))
    fresh_values, running, weights = corrected(key_rows, values, write_rate, log_decay, committed)
    result = readout(queries, key_rows, fresh_values, running, weights, committed)
    normed = result * lax.rsqrt(jnp.mean(result * result, -1, keepdims=True) + norm_eps) * head_gain
    gated = normed * jax.nn.silu(by_head(proj_gate, value_width))
    gated_rows = (
        jnp.transpose(gated, (0, 2, 1, 3))
        .reshape(seq_count * proposals, head_count * value_width)
        .astype(jnp.bfloat16)
    )
    return (gated_rows, committed)


def per_device(
    hidden,
    norm_gain,
    w_query,
    w_key,
    w_value,
    w_gate,
    w_write,
    w_decay,
    w_out,
    decay_rate,
    head_gain,
    carried_state,
    last_keys,
    last_values,
    last_writes,
    last_decays,
    accepted,
):
    local_width = hidden.shape[1]
    weight_set = (w_query, w_key, w_value, w_gate, w_write, w_decay)
    wide_rows = hidden.astype(jnp.float32)
    local_sq = jnp.sum(wide_rows * wide_rows, -1)
    gain_part = lax.dynamic_slice_in_dim(norm_gain, lax.axis_index("kv") * local_width, local_width)
    scaled = (wide_rows * gain_part.astype(jnp.float32)).astype(jnp.bfloat16)
    terms = tuple(
        (jnp.dot(scaled, weight, preferred_element_type=jnp.float32) for weight in weight_set)
    )
    summed = (
        lax.psum_scatter(
            terms[0].astype(jnp.bfloat16), "kv", scatter_dimension=0, tiled=True
        ).astype(jnp.float32),
        lax.psum_scatter(
            terms[1].astype(jnp.bfloat16), "kv", scatter_dimension=0, tiled=True
        ).astype(jnp.float32),
        lax.psum_scatter(
            terms[2].astype(jnp.bfloat16), "kv", scatter_dimension=0, tiled=True
        ).astype(jnp.float32),
        lax.psum_scatter(
            terms[3].astype(jnp.bfloat16), "kv", scatter_dimension=0, tiled=True
        ).astype(jnp.float32),
        lax.psum_scatter(
            terms[4].astype(jnp.bfloat16), "kv", scatter_dimension=0, tiled=True
        ).astype(jnp.float32),
        lax.psum_scatter(
            terms[5].astype(jnp.bfloat16), "kv", scatter_dimension=0, tiled=True
        ).astype(jnp.float32),
        lax.psum_scatter(
            local_sq.astype(jnp.bfloat16), "kv", scatter_dimension=0, tiled=True
        ).astype(jnp.float32),
    )
    projected = summed[:6]
    own_sq = summed[6]
    inverse = lax.rsqrt(own_sq / D + norm_eps)[:, None]
    normal_proj = tuple((matrix * inverse for matrix in projected))
    gated_rows, committed = core(
        normal_proj[0],
        normal_proj[1],
        normal_proj[2],
        normal_proj[3],
        normal_proj[4],
        normal_proj[5],
        decay_rate,
        head_gain,
        carried_state,
        last_keys,
        last_values,
        last_writes,
        last_decays,
        accepted,
    )
    partial_out = jnp.dot(
        lax.all_gather(gated_rows, "kv", axis=0, tiled=True),
        w_out,
        preferred_element_type=jnp.float32,
    )
    mixed_out = lax.psum_scatter(
        partial_out.astype(jnp.bfloat16), "tp", scatter_dimension=0, tiled=True
    )
    return (mixed_out, committed)


def solution(mesh):
    return jax.shard_map(
        per_device,
        mesh=mesh,
        in_specs=(
            P(None, "kv"),
            P(),
            P("kv", "tp"),
            P("kv", "tp"),
            P("kv", "tp"),
            P("kv", "tp"),
            P("kv", "tp"),
            P("kv", "tp"),
            P("tp", "kv"),
            P("tp"),
            P(),
            P("kv", "tp", None, None),
            P("kv", None, "tp"),
            P("kv", None, "tp"),
            P("kv", None, "tp"),
            P("kv", None, "tp"),
            P("kv"),
        ),
        out_specs=(P("tp", "kv"), P("kv", "tp", None, None)),
        check_vma=False,
    )
```

profile of v0, /device:TPU:0, one launch (start us, length us, event | category | flops | bytes accessed | tf_op | source)
XLA Modules:
  0.0 515.2 jit_solution(4329792237535709631)
XLA Ops:
  8.1 1.3 convolution_convert_fusion.5
  10.3 1.3 convolution_convert_fusion.6
  12.5 3.1 convolution_convert_fusion.2
  15.7 2.9 convolution_convert_fusion.3
  18.7 2.6 convolution_convert_fusion.1
  21.3 4.2 convolution_convert_fusion
  25.9 23.3 %all-reduce = bf16[512]{0:T(512)(128)(2,1)S(1)} all-reduce(bf16[512]{0:T(512)(128)(2,1)S(1)} %fusion.3), channel_id=3, replica_groups=mesh['kv'=8,'tp'=4] {'kv'}, use_global_device_ids=true, to_apply=%region_2.0.clone | all-reduce | flops 512 | bytes 2048
  51.5 24.9 %reduce-scatter.24.cloned.1.call-done = bf16[64,8]{1,0:T(8,128)(2,1)} async-done(((bf16[512,8]{1,0:T(8,128)(2,1)}), bf16[64,8]{1,0:T(8,128)(2,1)}) %reduce-scatter.24.cloned.1.call-update) | async-done | bytes 1040
  77.2 64.0 %reduce-scatter.22.cloned.1.call-done = bf16[64,8]{1,0:T(8,128)(2,1)} async-done(((bf16[512,8]{1,0:T(8,128)(2,1)}), bf16[64,8]{1,0:T(8,128)(2,1)}) %reduce-scatter.22.cloned.1.call-update) | async-done | bytes 1040
  144.7 1.5 fusion.1
  148.1 0.9 copy.295
  150.2 1.4 multiply_subtract_fusion.2
  152.4 10.9 %convolution_subtract_fusion.1 = f32[16,8,4,256]{3,2,1,0:T(4,128)S(1)} fusion(f32[16,8,128,256]{3,2,1,0:T(8,128)} %param.28, f32[16,8,4,384]{3,2,1,0:T(4,128)S(1)} %pad_maximum_fusion, f32[16,8,1,384]{3,2,1,0:T(1,128)S(1)} %get-tuple-element.6, f32[16,8,1,384]{3,2,1,0:T(1,128)S(1)} %get-tuple-element.7, f32[16,8,1,384]{3,2,1,0:T(1,128)S(1)} %get-tuple-element.8, ...), kind=kOutput, calls=%fused_computation.9 | convolution fusion | flops 201654272 | bytes 18612224 | tf_op jit(solution)/shard_map/bhcd,bhde->bhce/dot_general | solution.py:37
  163.2 21.7 %multiply_add_fusion = f32[16,8,128,256]{3,2,1,0:T(8,128)} fusion(f32[16,8,128,256]{3,2,1,0:T(8,128)} %param.28, f32[16,8,4,256]{3,2,1,0:T(4,128)S(1)} %convolution_subtract_fusion.1, f32[16,8]{1,0:T(8,128)S(1)} %copy.267, bf16[16,4,1024]{2,1,0:T(4,128)(2,1)S(1)} %copy-done.1, f32[16,8,4]{2,1,0:T(8,128)S(1)} %copy.269, f32[16,8,4]{2,1,0:T(8,128)S(1)} %add_rsqrt_fusion.1), kind=kOutput, calls=%fused_computation | convolution fusion | flops 209911808 | bytes 34214400 | tf_op jit(solution)/shard_map/bhcd,bhce->bhde/dot_general | solution.py:45
  184.9 22.9 %reduce-scatter.14.cloned.1.call-done = bf16[64,1024]{1,0:T(8,128)(2,1)} async-done(((bf16[512,1024]{1,0:T(8,128)(2,1)}), bf16[64,1024]{1,0:T(8,128)(2,1)}) %reduce-scatter.14.cloned.1.call-update) | async-done | bytes 131088 | tf_op jit(solution)/shard_map/reduce_scatter | solution.py:144
  207.9 66.4 %reduce-scatter.12.cloned.1.call-done = bf16[64,1024]{1,0:T(8,128)(2,1)} async-done(((bf16[512,1024]{1,0:T(8,128)(2,1)}), bf16[64,1024]{1,0:T(8,128)(2,1)}) %reduce-scatter.12.cloned.1.call-update) | async-done | bytes 131088 | tf_op jit(solution)/shard_map/reduce_scatter | solution.py:141
  274.3 1.2 multiply_bitcast_fusion
  276.7 1.7 fusion
  281.7 1.3 multiply_multiply_fusion
  283.1 2.8 convolution_multiply_fusion.1
  285.9 10.7 %fusion.33 = f32[16,8,4,256]{3,2,1,0:T(4,128)S(1)} fusion(f32[16,8,128,256]{3,2,1,0:T(8,128)} %multiply_add_fusion, f32[16,4,8,128]{3,2,1,0:T(8,128)S(1)} %bitcast.159, f32[16,8,4]{2,1,0:T(8,128)S(1)} %copy.264, f32[16,8,4]{2,1,0:T(8,128)S(1)} %get-tuple-element.35), kind=kOutput, calls=%fused_computation.76 | convolution fusion | flops 201457664 | bytes 17567744 | tf_op jit(solution)/shard_map/bhcd,bhde->bhce/dot_general | solution.py:52
  296.7 48.3 %reduce-scatter.16.cloned.1.call-done = bf16[64,2048]{1,0:T(8,128)(2,1)} async-done(((bf16[512,2048]{1,0:T(8,128)(2,1)}), bf16[64,2048]{1,0:T(8,128)(2,1)}) %reduce-scatter.16.cloned.1.call-update) | async-done | bytes 262160 | tf_op jit(solution)/shard_map/reduce_scatter | solution.py:147
  345.0 70.8 %reduce-scatter.18.cloned.1.call-done = bf16[64,2048]{1,0:T(8,128)(2,1)} async-done(((bf16[512,2048]{1,0:T(8,128)(2,1)}), bf16[64,2048]{1,0:T(8,128)(2,1)}) %reduce-scatter.18.cloned.1.call-update) | async-done | bytes 262160 | tf_op jit(solution)/shard_map/reduce_scatter | solution.py:150
  415.8 1.3 divide_multiply_fusion
  417.1 1.0 copy.332
  418.5 1.5 multiply_subtract_fusion
  420.8 10.9 %convolution_subtract_fusion = f32[16,8,4,256]{3,2,1,0:T(4,128)S(1)} fusion(f32[16,8,128,256]{3,2,1,0:T(8,128)} %multiply_add_fusion, f32[16,8,4,384]{3,2,1,0:T(4,128)S(1)} %pad_maximum_fusion.1, f32[16,8,1,384]{3,2,1,0:T(1,128)S(1)} %get-tuple-element.2, f32[16,8,1,384]{3,2,1,0:T(1,128)S(1)} %get-tuple-element.3, ...), kind=kOutput, calls=%fused_computation.8 | convolution fusion | flops 201654272 | bytes 18612224 | tf_op jit(solution)/shard_map/bhcd,bhde->bhce/dot_general | solution.py:37
  431.7 1.0 fusion.90
  433.4 1.3 fusion.7
  435.5 48.2 %all-gather.2.cloned.1.call-done = bf16[512,2048]{1,0:T(8,128)(2,1)} async-done(((bf16[64,2048]{1,0:T(8,128)(2,1)}), bf16[512,2048]{1,0:T(8,128)(2,1)}) %all-gather.2.cloned.1.call-update) | async-done | bytes 2097168 | tf_op jit(solution)/shard_map/all_gather | solution.py:184
  483.7 4.3 convolution_convert_fusion.4
  488.0 20.4 %reduce-scatter.20.cloned.1.call-done = bf16[128,512]{1,0:T(8,128)(2,1)} async-done(((bf16[512,512]{1,0:T(8,128)(2,1)}), bf16[128,512]{1,0:T(8,128)(2,1)}) %reduce-scatter.20.cloned.1.call-update) | async-done | bytes 131088 | tf_op jit(solution)/shard_map/reduce_scatter | solution.py:188
  (126 shorter events, 19.8 us)
Async XLA Ops:
  7.2 11.5 %copy-start = (bf16[512,2048]{1,0:T(8,128)(2,1)S(1)}, bf16[512,2048]{1,0:T(8,128)(2,1)}, u32[]{:S(2)}) copy-start(bf16[512,2048]{1,0:T(8,128)(2,1)} %param.21) | copy-start | bytes 6291460
  7.2 69.3 %reduce-scatter.24.cloned.1.call-start = ((), (), s32[]{:S(2)}) async-start(), calls=%async_computation.14 | async-start | bytes 147456
  10.2 131.0 %reduce-scatter.22.cloned.1.call-start = ((), (), s32[]{:S(2)}) async-start(), calls=%async_computation.13 | async-start | bytes 147456
  12.4 3.3 copy-start.2
  12.4 195.5 %reduce-scatter.14.cloned.1.call-start = ((), (), s32[]{:S(2)}) async-start(), calls=%async_computation.8 | async-start | bytes 1179648 | tf_op jit(solution)/shard_map/reduce_scatter | solution.py:144
  15.6 258.7 %reduce-scatter.12.cloned.1.call-start = ((), (), s32[]{:S(2)}) async-start(), calls=%async_computation.7 | async-start | bytes 1179648 | tf_op jit(solution)/shard_map/reduce_scatter | solution.py:141
  18.6 326.4 %reduce-scatter.16.cloned.1.call-start = ((), (), s32[]{:S(2)}) async-start(), calls=%async_computation.9 | async-start | bytes 2359296 | tf_op jit(solution)/shard_map/reduce_scatter | solution.py:147
  21.3 394.5 %reduce-scatter.18.cloned.1.call-start = ((), (), s32[]{:S(2)}) async-start(), calls=%async_computation.10 | async-start | bytes 2359296 | tf_op jit(solution)/shard_map/reduce_scatter | solution.py:150
  25.5 23.7 %copy-start.10 = (f32[16,4,8]{0,2,1:T(8,128)S(1)}, f32[16,4,8]{0,2,1:T(8,128)}, u32[]{:S(2)}) copy-start(f32[16,4,8]{0,2,1:T(8,128)} %param.32) | copy-start | bytes 6148
  25.5 23.8 %copy-start.17 = (s32[16]{0:T(128)S(1)}, s32[16]{0:T(128)}, u32[]{:S(2)}) copy-start(s32[16]{0:T(128)} %param.33) | copy-start | bytes 196
  25.5 23.8 %copy-start.18 = (f32[8]{0:T(128)S(1)}, f32[8]{0:T(128)}, u32[]{:S(2)}) copy-start(f32[8]{0:T(128)} %param.26) | copy-start | bytes 100
  25.5 23.9 %copy-start.11 = (f32[16,4,8]{0,2,1:T(8,128)S(1)}, f32[16,4,8]{0,2,1:T(8,128)}, u32[]{:S(2)}) copy-start(f32[16,4,8]{0,2,1:T(8,128)} %param.31) | copy-start | bytes 6148
  25.5 24.1 %copy-start.1 = (bf16[16,4,1024]{2,1,0:T(4,128)(2,1)S(1)}, bf16[16,4,1024]{2,1,0:T(4,128)(2,1)}, u32[]{:S(2)}) copy-start(bf16[16,4,1024]{2,1,0:T(4,128)(2,1)} %param.29) | copy-start | bytes 393220
  25.5 24.3 %copy-start.19 = (u32[32]{0:T(128)S(1)}, u32[32]{0:T(128)}, u32[]{:S(2)}) copy-start(u32[32]{0:T(128)} %constant.48) | copy-start | bytes 388
  25.6 25.8 %copy-start.4 = (bf16[16,4,2048]{2,1,0:T(4,128)(2,1)S(1)}, bf16[16,4,2048]{2,1,0:T(4,128)(2,1)}, u32[]{:S(2)}) copy-start(bf16[16,4,2048]{2,1,0:T(4,128)(2,1)} %param.30) | copy-start | bytes 786436
  25.6 458.1 %all-gather.2.cloned.1.call-start = ((), (), s32[]{:S(2)}) async-start(), calls=%async_computation.11 | async-start | bytes 2359296 | tf_op jit(solution)/shard_map/all_gather | solution.py:184
  25.8 120.4 %copy-start.20 = (pred[4,4]{1,0:T(4,128)(4,1)}, pred[4,4]{1,0:T(4,128)(4,1)S(1)}, u32[]{:S(2)}) copy-start(pred[4,4]{1,0:T(4,128)(4,1)S(1)} %iota_compare_fusion.2) | copy-start | bytes 52
  25.9 120.4 %copy-start.14 = (f32[4,4]{1,0:T(4,128)}, f32[4,4]{1,0:T(4,128)S(1)}, u32[]{:S(2)}) copy-start(f32[4,4]{1,0:T(4,128)S(1)} %convert_subtract_fusion) | copy-start | bytes 196
  51.3 223.0 %copy-start.12 = (f32[64]{0:T(128)}, f32[64]{0:T(128)S(1)}, u32[]{:S(2)}) copy-start(f32[64]{0:T(128)S(1)} %fusion.80) | copy-start | bytes 772
  184.9 91.7 %copy-start.6 = (f32[16,8,4]{2,1,0:T(8,128)S(1)}, f32[16,8,4]{2,1,0:T(8,128)}, u32[]{:S(2)}) copy-start(f32[16,8,4]{2,1,0:T(8,128)} %copy.289) | copy-start | bytes 6148
  184.9 91.7 %copy-start.15 = (f32[4,4]{1,0:T(4,128)S(1)}, f32[4,4]{1,0:T(4,128)}, u32[]{:S(2)}) copy-start(f32[4,4]{1,0:T(4,128)} %copy-done.14) | copy-start | bytes 196
  184.9 91.7 %copy-start.21 = (pred[4,4]{1,0:T(4,128)(4,1)S(1)}, pred[4,4]{1,0:T(4,128)(4,1)}, u32[]{:S(2)}) copy-start(pred[4,4]{1,0:T(4,128)(4,1)} %copy-done.20) | copy-start | bytes 52
  276.0 0.6 copy-start.5
  285.9 129.9 %copy-start.13 = (f32[64]{0:T(128)S(1)}, f32[64]{0:T(128)}, u32[]{:S(2)}) copy-start(f32[64]{0:T(128)} %copy-done.12) | copy-start | bytes 772
  296.6 121.9 %copy-start.7 = (f32[16,8,1,1]{1,0,2,3:T(8,128)S(1)}, f32[16,8,1,1]{1,0,2,3:T(8,128)}, u32[]{:S(2)}) copy-start(f32[16,8,1,1]{1,0,2,3:T(8,128)} %copy.322) | copy-start | bytes 1540
  296.6 121.9 %copy-start.8 = (f32[16,8,1,1]{1,0,2,3:T(8,128)S(1)}, f32[16,8,1,1]{1,0,2,3:T(8,128)}, u32[]{:S(2)}) copy-start(f32[16,8,1,1]{1,0,2,3:T(8,128)} %copy.321) | copy-start | bytes 1540
  296.7 121.9 %copy-start.9 = (f32[16,8,1,1]{1,0,2,3:T(8,128)S(1)}, f32[16,8,1,1]{1,0,2,3:T(8,128)}, u32[]{:S(2)}) copy-start(f32[16,8,1,1]{1,0,2,3:T(8,128)} %copy.320) | copy-start | bytes 1540
  420.8 10.9 %copy-start.3 = (f32[16,8,4,4]{3,2,1,0:T(4,128)S(1)}, f32[16,8,4,4]{3,2,1,0:T(4,128)}, u32[]{:S(2)}) copy-start(f32[16,8,4,4]{3,2,1,0:T(4,128)} %convolution_multiply_fusion.1) | copy-start | bytes 24580
  431.7 1.7 copy-start.16
  435.4 73.0 %reduce-scatter.20.cloned.1.call-start = ((), (), s32[]{:S(2)}) async-start(), calls=%async_computation.12 | async-start | bytes 655360 | tf_op jit(solution)/shard_map/reduce_scatter | solution.py:188
Sparse Core Ops, SparseCore 0:
  11.9 64.5 reduce-scatter.23
  80.3 60.8 reduce-scatter.21
  144.6 63.1 reduce-scatter.13
  211.1 63.0 reduce-scatter.11
  277.6 67.3 reduce-scatter.15
  348.4 67.3 reduce-scatter.17
  435.6 48.1 all-gather.1
  488.2 20.1 reduce-scatter.19
where the time goes:
time: 516 us; the launch traced here: 515 us
  waiting for transfers between devices  366 us (71%)
  matrix products  80.9 us (16%)
  blocking collectives  23.3 us (5%)
  local copies, waits for them, and re-layouts  15.7 us (3%)
  between operations  15.3 us (3%)
  other arithmetic  13.5 us (3%)
    unnamed x10, waiting for transfers between devices  89.1 us
    reduce_scatter x1, waiting for transfers between devices, per_device(): lax.psum_scatter(terms[3].astype(jnp.bfloat16), 'kv', scatter_dimension=0...  70.8 us
    reduce_scatter x1, waiting for transfers between devices, per_device(): lax.psum_scatter(terms[0].astype(jnp.bfloat16), 'kv', scatter_dimension=0...  66.4 us
    reduce_scatter x1, waiting for transfers between devices, per_device(): lax.psum_scatter(terms[2].astype(jnp.bfloat16), 'kv', scatter_dimension=0...  48.3 us
    all_gather x1, waiting for transfers between devices, per_device(): lax.all_gather(gated_rows, 'kv', axis=0, tiled=True)  48.2 us
    unnamed x1, blocking collectives  23.3 us
    reduce_scatter x1, waiting for transfers between devices, per_device(): lax.psum_scatter(terms[1].astype(jnp.bfloat16), 'kv', scatter_dimension=0...  22.9 us
    dot_general x2, matrix products, corrected(): jnp.einsum('bhcd,bhde->bhce', solved[..., value_width:], start_state, pre...  21.7 us
  transfers between devices with their start and end apart: 8, of which 8 were waited for; matrix products, arithmetic and copies ran while one was open for 16% of the time, Pallas kernels for 0%

commit v1 on v0

v1 whole, which is shorter than its diff:
```python
import functools
import jax
import jax.numpy as jnp
from jax import lax
from jax.experimental import pallas as pl
from jax.experimental.pallas import tpu as pltpu
from jax.sharding import PartitionSpec as P

norm_eps = 1e-06
LANES = 128
MESH = pl.DeviceIdType.MESH
VMEM_LIMIT = 60 * 1024 * 1024


def remote(src, dst, send, recv, device):
    return pltpu.make_async_remote_copy(
        src_ref=src, dst_ref=dst, send_sem=send, recv_sem=recv,
        device_id=device, device_id_type=MESH,
    )


def project_kernel(
    nx, nz, plan, width, sq_col, s_ref, small_ref, wq, wk, wv, wg, out_ref, small_out,
    wbuf, own, xs, xr, zs, zr, sm_xr, sm_zs, sm_zr,
    wsem, xss, xrs, zss, zrs, sxs, sxr, szs, szr,
):
    kv, tp = lax.axis_index("kv"), lax.axis_index("tp")
    x, z = lax.rem(kv, nx), lax.div(kv, nx)
    weights = (wq, wk, wv, wg)
    nc = len(plan)
    rows, cw = out_ref.shape[1], out_ref.shape[2]
    x_at = [lax.rem(x + d, nx) for d in range(nx)]
    z_at = [lax.rem(z + d, nz) for d in range(nz)]

    def fetch(c):
        which, off = plan[c]
        return pltpu.make_async_copy(
            weights[which].at[:, pl.ds(off, cw)], wbuf.at[c], wsem.at[c]
        )

    for c in range(nc):
        fetch(c).start()
    barrier = pltpu.get_barrier_semaphore()
    for d in range(1, nx):
        pl.semaphore_signal(barrier, inc=1, device_id=(z * nx + x_at[d], tp), device_id_type=MESH)
    for d in range(1, nz):
        pl.semaphore_signal(barrier, inc=1, device_id=(z_at[d] * nx + x, tp), device_id_type=MESH)
    pl.semaphore_wait(barrier, nx - 1 + nz - 1)

    def small_x(d):
        return remote(small_ref.at[x_at[d]], sm_xr.at[d - 1], sxs.at[d - 1], sxr.at[d - 1],
                      (z * nx + x_at[d], tp))

    def small_z(d):
        return remote(sm_zs.at[z_at[d]], sm_zr.at[d - 1], szs.at[d - 1], szr.at[d - 1],
                      (z_at[d] * nx + x, tp))

    def big_x(c, d):
        return remote(xs.at[c, d - 1], xr.at[c, d - 1], xss.at[c, d - 1], xrs.at[c, d - 1],
                      (z * nx + x_at[d], tp))

    def big_z(c, d):
        return remote(zs.at[c, z_at[d]], zr.at[c, d - 1], zss.at[c, d - 1], zrs.at[c, d - 1],
                      (z_at[d] * nx + x, tp))

    z_order = sorted(range(1, nz), key=lambda d: -min(d, nz - d))
    for d in range(1, nx):
        small_x(d).start()

    def multiply(c, carry):
        pltpu.make_async_copy(wbuf.at[c], wbuf.at[c], wsem.at[c]).wait()
        for d in range(1, nx):
            part = jnp.dot(s_ref[x_at[d]], wbuf[c], preferred_element_type=jnp.float32)
            xs[c, d - 1] = part.astype(jnp.bfloat16).reshape(nz, rows, cw)
            big_x(c, d).start()
        own[c] = jnp.dot(
            s_ref[x], wbuf[c], preferred_element_type=jnp.float32
        ).reshape(nz, rows, cw)
        return carry

    lax.fori_loop(0, nc, multiply, 0)

    total = small_ref[x].astype(jnp.float32)
    for d in range(1, nx):
        small_x(d).wait()
        total = total + sm_xr[d - 1].astype(jnp.float32)
    sm_zs[...] = total.astype(jnp.bfloat16)
    for d in z_order:
        small_z(d).start()

    def middle(c, carry):
        summed = own[c]
        for d in range(1, nx):
            big_x(c, d).wait()
            summed = summed + xr[c, d - 1].astype(jnp.float32)
        own[c] = summed
        zs[c] = summed.astype(jnp.bfloat16)
        for d in z_order:
            big_z(c, d).start()
        return carry

    lax.fori_loop(0, nc, middle, 0)

    small = sm_zs[z].astype(jnp.float32)
    for d in range(1, nz):
        small_z(d).wait()
        small = small + sm_zr[d - 1].astype(jnp.float32)
    inverse = lax.rsqrt(small[:, sq_col:sq_col + 1] / width + norm_eps)
    small_out[...] = small * inverse

    def finish(c, carry):
        summed = own[c, z]
        for d in range(1, nz):
            big_z(c, d).wait()
            summed = summed + zr[c, d - 1].astype(jnp.float32)
        out_ref[c] = summed * inverse
        return carry

    lax.fori_loop(0, nc, finish, 0)


def project(nx, nz, scaled, small, weights, sq_col, width):
    depth = scaled.shape[1]
    rows = scaled.shape[0] // (nx * nz)
    cw = min(512, weights[0].shape[1])
    plan = [(i, off) for i, w in enumerate(weights) for off in range(0, w.shape[1], cw)]
    nc = len(plan)
    by_x = jnp.transpose(scaled.reshape(nz, nx, rows, depth), (1, 0, 2, 3))
    by_x = by_x.reshape(nx, nz * rows, depth)
    small_x = jnp.transpose(small.reshape(nz, nx, rows, LANES), (1, 0, 2, 3))
    bf, f32, dma = jnp.bfloat16, jnp.float32, pltpu.SemaphoreType.DMA
    px, pz = max(nx - 1, 1), max(nz - 1, 1)
    vmem = pl.BlockSpec(memory_space=pltpu.VMEM)
    hbm = pl.BlockSpec(memory_space=pl.ANY)
    return plan, pl.pallas_call(
        functools.partial(project_kernel, nx, nz, plan, width, sq_col),
        out_shape=(
            jax.ShapeDtypeStruct((nc, rows, cw), f32),
            jax.ShapeDtypeStruct((rows, LANES), f32),
        ),
        in_specs=[vmem, vmem, hbm, hbm, hbm, hbm],
        out_specs=(vmem, vmem),
        scratch_shapes=[
            pltpu.VMEM((nc, depth, cw), bf),
            pltpu.VMEM((nc, nz, rows, cw), f32),
            pltpu.VMEM((nc, px, nz, rows, cw), bf),
            pltpu.VMEM((nc, px, nz, rows, cw), bf),
            pltpu.VMEM((nc, nz, rows, cw), bf),
            pltpu.VMEM((nc, pz, rows, cw), bf),
            pltpu.VMEM((px, nz, rows, LANES), bf),
            pltpu.VMEM((nz, rows, LANES), bf),
            pltpu.VMEM((pz, rows, LANES), bf),
            dma((nc,)),
            dma((nc, px)), dma((nc, px)), dma((nc, pz)), dma((nc, pz)),
            dma((px,)), dma((px,)), dma((pz,)), dma((pz,)),
        ],
        compiler_params=pltpu.CompilerParams(
            collective_id=0, has_side_effects=True, vmem_limit_bytes=VMEM_LIMIT
        ),
    )(by_x, small_x, *weights)


def silu(v):
    return v * jax.nn.sigmoid(v)


def unit(v):
    return v * lax.rsqrt(jnp.sum(v * v, -1, keepdims=True) + norm_eps)


def solve(keys, values, write, decay):
    steps = len(keys)
    running = [decay[0]]
    for t in range(1, steps):
        running.append(running[-1] + decay[t])
    strong = [keys[t] * write[t] for t in range(steps)]
    u_val, u_key = [], []
    for t in range(steps):
        cur_v = values[t] * write[t]
        cur_k = strong[t] * jnp.exp(running[t])
        for s in range(t):
            low = jnp.sum(strong[t] * keys[s], -1, keepdims=True)
            low = low * jnp.exp(running[t] - running[s])
            cur_v = cur_v - low * u_val[s]
            cur_k = cur_k - low * u_key[s]
        u_val.append(cur_v)
        u_key.append(cur_k)
    return running, u_val, u_key


def core_kernel(
    heads, q_ref, k_ref, v_ref, g_ref, small_ref, lk_ref, lv_ref, lsmall_ref, rate_ref,
    gain_ref, state_ref, gated_ref, com_ref, left, prod, kd, fr, dec, wide_k, wide_v, gout,
):
    h = pl.program_id(0)
    seqs = state_ref.shape[0]
    steps = q_ref.shape[1] // seqs
    dk, dv = q_ref.shape[2], v_ref.shape[2]
    pad = left.shape[1]
    bf, f32 = jnp.bfloat16, jnp.float32

    def at_t(ref, t):
        return ref[pl.ds(t, seqs, stride=steps), :]

    tiles = dv // LANES

    def value_at(ref, t):
        return jnp.concatenate([at_t(ref.at[j], t) for j in range(tiles)], -1)

    def cut(j):
        return slice(j * LANES, (j + 1) * LANES)

    lane = lax.broadcasted_iota(jnp.int32, (seqs, LANES), 1)

    def column(mat, col):
        return jnp.sum(jnp.where(lane == col, mat, 0.0), -1, keepdims=True)

    rate = column(jnp.broadcast_to(rate_ref[...], (seqs, LANES)), h)
    every = range(steps)

    wide_k[...] = lk_ref[...].astype(f32)
    for j in range(tiles):
        wide_v[j] = lv_ref[:, cut(j)].astype(f32)
    old = [at_t(lsmall_ref, t) for t in every]
    taken = [column(m, 2 * heads) for m in old]
    write = [jax.nn.sigmoid(column(old[t], h)) * taken[t] for t in every]
    decay = [-rate * jax.nn.softplus(column(old[t], heads + h)) * taken[t] for t in every]
    keys = [unit(at_t(wide_k, t)) for t in every]
    running, u_val, u_key = solve(keys, [value_at(wide_v, t) for t in every], write, decay)
    for t in every:
        left[:, t, :] = u_key[t]
        kd[:, t, :] = keys[t] * jnp.exp(running[-1] - running[t])
    dec[...] = jnp.broadcast_to(jnp.exp(running[-1]), (seqs, dv))
    for t in range(steps, pad):
        left[:, t, :] = jnp.zeros((seqs, dk), f32)
        kd[:, t, :] = jnp.zeros((seqs, dk), f32)
        fr[:, t, :] = jnp.zeros((seqs, dv), f32)
    for b in range(seqs):
        prod[b] = jnp.dot(
            left[b].astype(bf), state_ref[b, 0].astype(bf), preferred_element_type=f32
        )
    for t in every:
        fr[:, t, :] = u_val[t] - prod[:, t, :]

    small = [at_t(small_ref, t) for t in every]
    write = [jax.nn.sigmoid(column(small[t], h)) for t in every]
    decay = [-rate * jax.nn.softplus(column(small[t], heads + h)) for t in every]
    queries = [unit(silu(at_t(q_ref.at[0], t))) * dk ** (-0.5) for t in every]
    for j in range(tiles):
        wide_v[j] = silu(v_ref[0, :, cut(j)])
    keys = [unit(silu(at_t(k_ref.at[0], t))) for t in every]
    running, u_val, u_key = solve(keys, [value_at(wide_v, t) for t in every], write, decay)
    for t in every:
        left[:, t, :] = u_key[t]
        left[:, steps + t, :] = queries[t] * jnp.exp(running[t])
    for b in range(seqs):
        added = lax.dot_general(
            kd[b].astype(bf), fr[b].astype(bf), (((0,), (0,)), ((), ())),
            preferred_element_type=f32,
        )
        after = state_ref[b, 0] * dec[b:b + 1, :] + added
        com_ref[b, 0] = after
        prod[b] = jnp.dot(left[b].astype(bf), after.astype(bf), preferred_element_type=f32)

    gain = gain_ref[...]
    fresh = [u_val[t] - prod[:, t, :] for t in every]
    for t in every:
        result = prod[:, steps + t, :]
        for s in range(t + 1):
            score = jnp.sum(queries[t] * keys[s], -1, keepdims=True)
            score = score * jnp.exp(running[t] - running[s])
            result = result + score * fresh[s]
        scale = lax.rsqrt(jnp.mean(result * result, -1, keepdims=True) + norm_eps)
        normed = result * scale * gain
        for j in range(tiles):
            gout[j, pl.ds(t, seqs, stride=steps), :] = normed[:, cut(j)]
    for j in range(tiles):
        gated_ref[:, cut(j)] = (gout[j] * silu(g_ref[0, :, cut(j)])).astype(bf)


def core(plan, projected, small, last_keys, last_values, last_small, rates, head_gain, state):
    seqs, heads, dk, dv = state.shape
    steps = last_keys.shape[1]
    rows = seqs * steps
    cw = projected.shape[2]
    kpc, vpc = cw // dk, cw // dv
    first = [next(c for c, (w, _) in enumerate(plan) if w == i) for i in range(4)]
    pad = 2 * steps
    f32 = jnp.float32

    def key_block(base):
        return pl.BlockSpec((1, rows, dk), lambda h: (base + h // kpc, 0, h % kpc))

    def val_block(base):
        return pl.BlockSpec((1, rows, dv), lambda h: (base + h // vpc, 0, h % vpc))

    def whole(shape):
        return pl.BlockSpec(shape, lambda h: (0,) * len(shape))

    state_block = pl.BlockSpec((seqs, 1, dk, dv), lambda h: (0, h, 0, 0))
    return pl.pallas_call(
        functools.partial(core_kernel, heads),
        grid=(heads,),
        out_shape=(
            jax.ShapeDtypeStruct((rows, heads * dv), jnp.bfloat16),
            jax.ShapeDtypeStruct(state.shape, f32),
        ),
        in_specs=[
            key_block(first[0]), key_block(first[1]), val_block(first[2]), val_block(first[3]),
            whole((rows, LANES)),
            pl.BlockSpec((rows, dk), lambda h: (0, h)),
            pl.BlockSpec((rows, dv), lambda h: (0, h)),
            whole((rows, LANES)), whole((1, LANES)), whole((1, dv)), state_block,
        ],
        out_specs=(pl.BlockSpec((rows, dv), lambda h: (0, h)), state_block),
        scratch_shapes=[
            pltpu.VMEM((seqs, pad, dk), f32),
            pltpu.VMEM((seqs, pad, dv), f32),
            pltpu.VMEM((seqs, pad, dk), f32),
            pltpu.VMEM((seqs, pad, dv), f32),
            pltpu.VMEM((seqs, dv), f32),
            pltpu.VMEM((rows, dk), f32),
            pltpu.VMEM((dv // LANES, rows, LANES), f32),
            pltpu.VMEM((dv // LANES, rows, LANES), f32),
        ],
        compiler_params=pltpu.CompilerParams(vmem_limit_bytes=VMEM_LIMIT),
    )(
        projected, projected, projected, projected, small,
        last_keys.reshape(rows, heads * dk), last_values.reshape(rows, heads * dv),
        last_small, rates, head_gain, state,
    )


def output_kernel(
    nx, nz, ntp, g_ref, w_ref, out_ref, held, parts, got,
    zss, zrs, xss, xrs, tss, trs, csem,
):
    kv, tp = lax.axis_index("kv"), lax.axis_index("tp")
    x, z = lax.rem(kv, nx), lax.div(kv, nx)
    rows = g_ref.shape[0]
    per = out_ref.shape[0]
    pieces = nx * rows // per
    x_at = [lax.rem(x + d, nx) for d in range(nx)]
    z_at = [lax.rem(z + d, nz) for d in range(nz)]
    z_from = [lax.rem(z + nz - d, nz) for d in range(nz)]
    x_from = [lax.rem(x + nx - d, nx) for d in range(nx)]
    t_at = [lax.rem(tp + d, ntp) for d in range(ntp)]

    barrier = pltpu.get_barrier_semaphore()
    for d in range(1, nx):
        pl.semaphore_signal(barrier, inc=1, device_id=(z * nx + x_at[d], tp), device_id_type=MESH)
    for d in range(1, nz):
        pl.semaphore_signal(barrier, inc=1, device_id=(z_at[d] * nx + x, tp), device_id_type=MESH)
    for d in range(1, ntp):
        pl.semaphore_signal(barrier, inc=1, device_id=(kv, t_at[d]), device_id_type=MESH)
    local = pltpu.make_async_copy(g_ref, held.at[z, x], csem)
    local.start()
    pl.semaphore_wait(barrier, nx - 1 + nz - 1 + ntp - 1)

    def along_z(d):
        return remote(g_ref, held.at[z, x], zss.at[d], zrs.at[d], (z_at[d] * nx + x, tp))

    def landed_z(k):
        return remote(g_ref, held.at[z_from[k], x], zss.at[k], zrs.at[k],
                      (z_at[k] * nx + x, tp))

    def along_x(k, d):
        return remote(held.at[z_from[k], x], held.at[z_from[k], x],
                      xss.at[k, d], xrs.at[k, d], (z * nx + x_at[d], tp))

    def landed_x(k, d):
        return remote(held.at[z_from[k], x], held.at[z_from[k], x_from[d]],
                      xss.at[k, d], xrs.at[k, d], (z * nx + x_at[d], tp))

    def own_x(d):
        return remote(g_ref, held.at[z, x], xss.at[0, d], xrs.at[0, d],
                      (z * nx + x_at[d], tp))

    for d in range(1, nz):
        along_z(d).start()
    for d in range(1, nx):
        own_x(d).start()
    local.wait()
    for k in range(nz):
        if k > 0:
            landed_z(k).wait_recv()
            for d in range(1, nx):
                along_x(k, d).start()

    def to_tp(block, j):
        target = block * pieces + j
        return target

    for k in range(nz):
        for d in range(1, nx):
            landed_x(k, d).wait_recv()
        block = z_from[k]
        product = jnp.dot(
            held[block].reshape(nx * rows, held.shape[3]), w_ref[...],
            preferred_element_type=jnp.float32,
        )
        for j in range(pieces):
            parts[block * pieces + j] = product[j * per:(j + 1) * per].astype(jnp.bfloat16)
            target = block * pieces + j

            @pl.when(target != tp)
            def _():
                remote(parts.at[target], got.at[tp], tss.at[target], trs.at[tp],
                       (kv, target)).start()

    summed = parts[tp].astype(jnp.float32)
    for d in range(1, ntp):
        source = t_at[d]
        remote(parts.at[source], got.at[source], tss.at[source], trs.at[source],
               (kv, source)).wait()
        summed = summed + got[source].astype(jnp.float32)
    out_ref[...] = summed.astype(out_ref.dtype)
    for d in range(1, nz):
        along_z(d).wait_send()
    for d in range(1, nx):
        own_x(d).wait_send()
        for k in range(1, nz):
            along_x(k, d).wait_send()


def output(nx, nz, ntp, gated, w_out):
    rows, depth = gated.shape
    columns = w_out.shape[1]
    per = rows * nx * nz // ntp
    bf, dma = jnp.bfloat16, pltpu.SemaphoreType.DMA
    vmem = pl.BlockSpec(memory_space=pltpu.VMEM)
    return pl.pallas_call(
        functools.partial(output_kernel, nx, nz, ntp),
        out_shape=jax.ShapeDtypeStruct((per, columns), bf),
        in_specs=[vmem, vmem],
        out_specs=vmem,
        scratch_shapes=[
            pltpu.VMEM((nz, nx, rows, depth), bf),
            pltpu.VMEM((ntp, per, columns), bf),
            pltpu.VMEM((ntp, per, columns), bf),
            dma((nz,)), dma((nz,)), dma((nz, nx)), dma((nz, nx)),
            dma((ntp,)), dma((ntp,)), dma(()),
        ],
        compiler_params=pltpu.CompilerParams(
            collective_id=1, has_side_effects=True, vmem_limit_bytes=VMEM_LIMIT
        ),
    )(gated, w_out)


def per_device(
    nkv, ntp, hidden, norm_gain, w_query, w_key, w_value, w_gate, w_write, w_decay, w_out,
    decay_rate, head_gain, carried_state, last_keys, last_values, last_writes, last_decays,
    accepted,
):
    f32 = jnp.float32
    nz = 4 if nkv % 4 == 0 else 1
    nx = nkv // nz
    local_width = hidden.shape[1]
    seqs, heads = carried_state.shape[:2]
    steps = last_keys.shape[1]
    rows = seqs * steps
    wide = hidden.astype(f32)
    local_sq = jnp.sum(wide * wide, -1, keepdims=True)
    gain = lax.dynamic_slice_in_dim(norm_gain, lax.axis_index("kv") * local_width, local_width)
    scaled = (wide * gain.astype(f32)).astype(jnp.bfloat16)
    w_small = jnp.concatenate([w_write, w_decay], 1)
    small = jnp.dot(scaled, w_small, preferred_element_type=f32)
    fill = LANES - 2 * heads - 1
    small = jnp.concatenate(
        [small, local_sq, jnp.zeros((small.shape[0], fill), f32)], 1
    ).astype(jnp.bfloat16)
    plan, (projected, small) = project(
        nx, nz, scaled, small, (w_query, w_key, w_value, w_gate), 2 * heads, local_width * nkv
    )
    taken = (jnp.arange(steps, dtype=jnp.int32)[None, :] < accepted[:, None]).astype(f32)
    last_small = jnp.concatenate(
        [last_writes.reshape(rows, heads), last_decays.reshape(rows, heads),
         taken.reshape(rows, 1), jnp.zeros((rows, fill), f32)], 1
    )
    rates = jnp.pad(decay_rate, (0, LANES - heads))[None, :]
    gated, committed = core(
        plan, projected, small, last_keys, last_values, last_small, rates,
        head_gain[None, :], carried_state,
    )
    return (output(nx, nz, ntp, gated, w_out), committed)


def solution(mesh):
    return jax.shard_map(
        functools.partial(per_device, mesh.shape["kv"], mesh.shape["tp"]),
        mesh=mesh,
        in_specs=(
            P(None, "kv"),
            P(),
            P("kv", "tp"),
            P("kv", "tp"),
            P("kv", "tp"),
            P("kv", "tp"),
            P("kv", "tp"),
            P("kv", "tp"),
            P("tp", "kv"),
            P("tp"),
            P(),
            P("kv", "tp", None, None),
            P("kv", None, "tp"),
            P("kv", None, "tp"),
            P("kv", None, "tp"),
            P("kv", None, "tp"),
            P("kv"),
        ),
        out_specs=(P("tp", "kv"), P("kv", "tp", None, None)),
        check_vma=False,
    )
```

time: 516 us -> 171 us (0.33)
  waiting for transfers between devices: 366 us -> 0 us
  Pallas kernels: 0 us -> 153 us
  matrix products: 80.9 us -> 0.23 us
  blocking collectives: 23.3 us -> 0 us
  between operations: 15.3 us -> 0.69 us
  other arithmetic: 13.5 us -> 4.22 us
  local copies, waits for them, and re-layouts: 15.7 us -> 9.25 us
    reduce_scatter x5 -> x0, waiting for transfers between devices: 229 us -> none  [the longest x1 70.8 us: per_device(): lax.psum_scatter(terms[3].astype(jnp.bfloat16), 'kv', scatter_dimension=0...]
    pallas_call x0 -> x3, Pallas kernels: none -> 153 us  [the longest x1 85.2 us: project(): pl.pallas_call(functools.partial(project_kernel, nx, nz, plan, width, sq_...]
    unnamed x10 -> x0, waiting for transfers between devices: 89.1 us -> none
    dot_general x15 -> x1, matrix products: 80.9 us -> 0.23 us  [per_device(): small = jnp.dot(scaled, w_small, preferred_element_type=f32)]
    all_gather x1 -> x0, waiting for transfers between devices: 48.2 us -> none  [per_device(): lax.all_gather(gated_rows, 'kv', axis=0, tiled=True)]
    unnamed x1 -> x0, blocking collectives: 23.3 us -> none
  transfers between devices with their start and end apart: 8 -> 0, of which waited for: 8 -> 0; matrix products, arithmetic and copies ran while one was open for 16% -> 0% of each run, Pallas kernels for 0% -> 0%
where the time goes in v1:
time: 171 us; the launch traced here: 167 us
  Pallas kernels  153 us (89%)
  local copies, waits for them, and re-layouts  9.25 us (5%)
  other arithmetic  4.22 us (2%)
    pallas_call x1, Pallas kernels, project(): pl.pallas_call(functools.partial(project_kernel, nx, nz, plan, width, sq_...  85.2 us
    pallas_call x1, Pallas kernels, output(): pl.pallas_call(functools.partial(output_kernel, nx, nz, ntp), out_shape=j...  38.8 us
    pallas_call x1, Pallas kernels, core(): pl.pallas_call(functools.partial(core_kernel, heads), grid=(heads,), out_...  28.9 us

profile of v1, /device:TPU:0, one launch (start us, length us, event | category | flops | bytes accessed | tf_op | source)
XLA Modules:
  0.0 167.3 jit_solution(12224848441436233085)
XLA Ops:
  0.6 0.0 copy-start
  0.6 0.0 copy-start.1
  0.7 1.2 pad_bitcast_fusion.rate_ref
  1.9 0.1 pad.8.clone
  1.9 0.1 pad.11.clone
  2.0 0.8 dynamic-slice_convert_fusion
  2.8 0.7 fusion.5
  3.5 0.1 reshape.66
  3.6 0.8 copy.26
  4.4 0.8 copy.27
  5.2 0.7 maximum_maximum_fusion.lsmall_ref
  5.9 1.6 reshape.61.lk_ref
  7.5 1.7 %reshape.62.lv_ref = bf16[64,2048]{1,0:T(8,128)(2,1)} reshape(bf16[16,4,2048]{2,1,0:T(4,128)(2,1)} %param.30) | data formatting | bytes 524288 | tf_op jit(solution)/shard_map/reshape | solution.py:329
  9.2 1.3 fusion.1
  10.5 0.1 concatenate.17
  10.5 0.0 copy-done
  10.5 0.0 copy-done.1
  10.5 0.2 convolution_convert_fusion
  10.8 0.1 concatenate.16
  10.9 0.1 copy.24
  11.0 0.2 copy.25
  11.2 0.8 maximum_bitcast_fusion.small_ref
  12.0 0.8 copy.23
  12.8 85.2 %shard_map.176 = (f32[12,64,512]{2,1,0:T(8,128)}, f32[64,128]{1,0:T(8,128)}) custom-call(bf16[2,256,512]{2,1,0:T(8,128)(2,1)} %bitcast.15, bf16[2,4,64,128]{3,2,1,0:T(8,128)(2,1)} %maximum_bitcast_fusion.small_ref, bf16[512,1024]{1,0:T(8,128)(2,1)} %wq.1, bf16[512,1024]{1,0:T(8,128)(2,1)} %wk.1, bf16[512,2048]{1,0:T(8,128)(2,1)} %wv.1, bf16[512,2048]{1,0:T(8,128)(2,1)} %wg.1), custom_call_target="tpu_custom_call" | custom-call | tf_op jit(solution)/shard_map/pallas_call | solution.py:135
  98.0 28.9 %shard_map.177 = (bf16[64,2048]{1,0:T(8,128)(2,1)}, f32[16,8,128,256]{3,2,1,0:T(8,128)}) custom-call(f32[12,64,512]{2,1,0:T(8,128)} %get-tuple-element.6.q_ref.k_ref.v_ref.g_ref, f32[12,64,512]{2,1,0:T(8,128)} %get-tuple-element.6.q_ref.k_ref.v_ref.g_ref, f32[12,64,512]{2,1,0:T(8,128)} %get-tuple-element.6.q_ref.k_ref.v_ref.g_ref, ...), custom_call_target="tpu_custom_call" | custom-call | tf_op jit(solution)/shard_map/pallas_call | solution.py:301
  126.9 38.8 %shard_map.178 = bf16[128,512]{1,0:T(8,128)(2,1)} custom-call(bf16[64,2048]{1,0:T(8,128)(2,1)} %get-tuple-element.8.g_ref, bf16[2048,512]{1,0:T(8,128)(2,1)} %w_ref.1), custom_call_target="tpu_custom_call" | custom-call | tf_op jit(solution)/shard_map/pallas_call | solution.py:432
  165.7 1.6 copy.30
  (2 shorter events, 0.0 us)
Async XLA Ops:
  0.6 9.9 %copy-start = (bf16[512,8]{0,1:T(8,128)(2,1)S(1)}, bf16[512,8]{0,1:T(8,128)(2,1)}, u32[]{:S(2)}) copy-start(bf16[512,8]{0,1:T(8,128)(2,1)} %param.24) | copy-start | bytes 24580
  0.6 9.9 %copy-start.1 = (bf16[512,8]{0,1:T(8,128)(2,1)S(1)}, bf16[512,8]{0,1:T(8,128)(2,1)}, u32[]{:S(2)}) copy-start(bf16[512,8]{0,1:T(8,128)(2,1)} %param.23) | copy-start | bytes 24580

commit v2 on v1

--- a/solution.py
+++ b/solution.py
@@ -20,8 +20,8 @@
 
 
 def project_kernel(
-    nx, nz, plan, width, sq_col, s_ref, small_ref, wq, wk, wv, wg, out_ref, small_out,
-    wbuf, own, xs, xr, zs, zr, sm_xr, sm_zs, sm_zr,
+    nx, nz, plan, width, sq_col, h_ref, n_ref, ws_ref, wq, wk, wv, wg, out_ref, small_out,
+    s_ref, small_ref, wbuf, own, xs, xr, zs, zr, sm_xr, sm_zs, sm_zr,
     wsem, xss, xrs, zss, zrs, sxs, sxr, szs, szr,
 ):
     kv, tp = lax.axis_index("kv"), lax.axis_index("tp")
@@ -45,6 +45,16 @@
         pl.semaphore_signal(barrier, inc=1, device_id=(z * nx + x_at[d], tp), device_id_type=MESH)
     for d in range(1, nz):
         pl.semaphore_signal(barrier, inc=1, device_id=(z_at[d] * nx + x, tp), device_id_type=MESH)
+    gain = n_ref[...].astype(jnp.float32)
+    lane = lax.broadcasted_iota(jnp.int32, (rows, LANES), 1)
+    for i in range(nx):
+        for j in range(nz):
+            wide = h_ref[(j * nx + i) * rows:(j * nx + i + 1) * rows].astype(jnp.float32)
+            scaled = (wide * gain).astype(jnp.bfloat16)
+            s_ref[i, j * rows:(j + 1) * rows] = scaled
+            part = jnp.dot(scaled, ws_ref[...], preferred_element_type=jnp.float32)
+            square = jnp.sum(wide * wide, -1, keepdims=True)
+            small_ref[i, j] = jnp.where(lane == sq_col, square, part).astype(jnp.bfloat16)
     pl.semaphore_wait(barrier, nx - 1 + nz - 1)
 
     def small_x(d):
@@ -119,15 +129,12 @@
     lax.fori_loop(0, nc, finish, 0)
 
 
-def project(nx, nz, scaled, small, weights, sq_col, width):
-    depth = scaled.shape[1]
-    rows = scaled.shape[0] // (nx * nz)
+def project(nx, nz, hidden, gain, w_small, weights, sq_col, width):
+    depth = hidden.shape[1]
+    rows = hidden.shape[0] // (nx * nz)
     cw = min(512, weights[0].shape[1])
     plan = [(i, off) for i, w in enumerate(weights) for off in range(0, w.shape[1], cw)]
     nc = len(plan)
-    by_x = jnp.transpose(scaled.reshape(nz, nx, rows, depth), (1, 0, 2, 3))
-    by_x = by_x.reshape(nx, nz * rows, depth)
-    small_x = jnp.transpose(small.reshape(nz, nx, rows, LANES), (1, 0, 2, 3))
     bf, f32, dma = jnp.bfloat16, jnp.float32, pltpu.SemaphoreType.DMA
     px, pz = max(nx - 1, 1), max(nz - 1, 1)
     vmem = pl.BlockSpec(memory_space=pltpu.VMEM)
@@ -138,9 +145,11 @@
             jax.ShapeDtypeStruct((nc, rows, cw), f32),
             jax.ShapeDtypeStruct((rows, LANES), f32),
         ),
-        in_specs=[vmem, vmem, hbm, hbm, hbm, hbm],
+        in_specs=[vmem, vmem, vmem, hbm, hbm, hbm, hbm],
         out_specs=(vmem, vmem),
         scratch_shapes=[
+            pltpu.VMEM((nx, nz * rows, depth), bf),
+            pltpu.VMEM((nx, nz, rows, LANES), bf),
             pltpu.VMEM((nc, depth, cw), bf),
             pltpu.VMEM((nc, nz, rows, cw), f32),
             pltpu.VMEM((nc, px, nz, rows, cw), bf),
@@ -157,7 +166,7 @@
         compiler_params=pltpu.CompilerParams(
             collective_id=0, has_side_effects=True, vmem_limit_bytes=VMEM_LIMIT
         ),
-    )(by_x, small_x, *weights)
+    )(hidden, gain, w_small, *weights)
 
 
 def silu(v):
@@ -189,8 +198,8 @@
 
 
 def core_kernel(
-    heads, q_ref, k_ref, v_ref, g_ref, small_ref, lk_ref, lv_ref, lsmall_ref, rate_ref,
-    gain_ref, state_ref, gated_ref, com_ref, left, prod, kd, fr, dec, wide_k, wide_v, gout,
+    heads, q_ref, k_ref, v_ref, g_ref, small_ref, lk_ref, lv_ref, lw_ref, ld_ref, acc_ref, rate_ref,
+    gain_ref, state_ref, gated_ref, com_ref, left, prod, kd, fr, dec, old_k, old_v, wide_v, gout,
 ):
     h = pl.program_id(0)
     seqs = state_ref.shape[0]
@@ -212,21 +221,22 @@
 
     lane = lax.broadcasted_iota(jnp.int32, (seqs, LANES), 1)
 
+    few = lax.broadcasted_iota(jnp.int32, (seqs, heads), 1)
+
     def column(mat, col):
-        return jnp.sum(jnp.where(lane == col, mat, 0.0), -1, keepdims=True)
-
-    rate = column(jnp.broadcast_to(rate_ref[...], (seqs, LANES)), h)
+        index = lane if mat.shape[1] == LANES else few
+        return jnp.sum(jnp.where(index == col, mat, 0.0), -1, keepdims=True)
+
+    rate = column(jnp.broadcast_to(rate_ref[...], (seqs, heads)), h)
     every = range(steps)
 
-    wide_k[...] = lk_ref[...].astype(f32)
-    for j in range(tiles):
-        wide_v[j] = lv_ref[:, cut(j)].astype(f32)
-    old = [at_t(lsmall_ref, t) for t in every]
-    taken = [column(m, 2 * heads) for m in old]
-    write = [jax.nn.sigmoid(column(old[t], h)) * taken[t] for t in every]
-    decay = [-rate * jax.nn.softplus(column(old[t], heads + h)) * taken[t] for t in every]
-    keys = [unit(at_t(wide_k, t)) for t in every]
-    running, u_val, u_key = solve(keys, [value_at(wide_v, t) for t in every], write, decay)
+    old_k[...] = lk_ref[...].astype(f32)
+    old_v[...] = lv_ref[...].astype(f32)
+    taken = [(acc_ref[...] > t).astype(f32) for t in every]
+    write = [jax.nn.sigmoid(column(lw_ref[:, t, :], h)) * taken[t] for t in every]
+    decay = [-rate * jax.nn.softplus(column(ld_ref[:, t, :], h)) * taken[t] for t in every]
+    keys = [unit(old_k[:, t, :]) for t in every]
+    running, u_val, u_key = solve(keys, [old_v[:, t, :] for t in every], write, decay)
     for t in every:
         left[:, t, :] = u_key[t]
         kd[:, t, :] = keys[t] * jnp.exp(running[-1] - running[t])
@@ -278,7 +288,8 @@
         gated_ref[:, cut(j)] = (gout[j] * silu(g_ref[0, :, cut(j)])).astype(bf)
 
 
-def core(plan, projected, small, last_keys, last_values, last_small, rates, head_gain, state):
+def core(plan, projected, small, last_keys, last_values, last_writes, last_decays, accepted,
+         rates, head_gain, state):
     seqs, heads, dk, dv = state.shape
     steps = last_keys.shape[1]
     rows = seqs * steps
@@ -308,9 +319,10 @@
         in_specs=[
             key_block(first[0]), key_block(first[1]), val_block(first[2]), val_block(first[3]),
             whole((rows, LANES)),
-            pl.BlockSpec((rows, dk), lambda h: (0, h)),
-            pl.BlockSpec((rows, dv), lambda h: (0, h)),
-            whole((rows, LANES)), whole((1, LANES)), whole((1, dv)), state_block,
+            pl.BlockSpec((seqs, steps, dk), lambda h: (0, 0, h)),
+            pl.BlockSpec((seqs, steps, dv), lambda h: (0, 0, h)),
+            whole((seqs, steps, heads)), whole((seqs, steps, heads)), whole((seqs, 1)),
+            whole((1, heads)), whole((1, dv)), state_block,
         ],
         out_specs=(pl.BlockSpec((rows, dv), lambda h: (0, h)), state_block),
         scratch_shapes=[
@@ -319,94 +331,130 @@
             pltpu.VMEM((seqs, pad, dk), f32),
             pltpu.VMEM((seqs, pad, dv), f32),
             pltpu.VMEM((seqs, dv), f32),
-            pltpu.VMEM((rows, dk), f32),
+            pltpu.VMEM((seqs, steps, dk), f32),
+            pltpu.VMEM((seqs, steps, dv), f32),
             pltpu.VMEM((dv // LANES, rows, LANES), f32),
             pltpu.VMEM((dv // LANES, rows, LANES), f32),
         ],
         compiler_params=pltpu.CompilerParams(vmem_limit_bytes=VMEM_LIMIT),
     )(
         projected, projected, projected, projected, small,
-        last_keys.reshape(rows, heads * dk), last_values.reshape(rows, heads * dv),
-        last_small, rates, head_gain, state,
+        last_keys, last_values, last_writes, last_decays, accepted, rates, head_gain, state,
     )
 
 
 def output_kernel(
-    nx, nz, ntp, g_ref, w_ref, out_ref, held, parts, got,
-    zss, zrs, xss, xrs, tss, trs, csem,
+    nx, nz, ntp, g_ref, w_hbm, out_ref, held, parts, got, w_ref,
+    zss, zrs, xss, xrs, tss, trs, csem, wsem,
 ):
     kv, tp = lax.axis_index("kv"), lax.axis_index("tp")
     x, z = lax.rem(kv, nx), lax.div(kv, nx)
-    rows = g_ref.shape[0]
+    halves, rows, depth = held.shape[2:]
     per = out_ref.shape[0]
     pieces = nx * rows // per
     x_at = [lax.rem(x + d, nx) for d in range(nx)]
-    z_at = [lax.rem(z + d, nz) for d in range(nz)]
-    z_from = [lax.rem(z + nz - d, nz) for d in range(nz)]
-    x_from = [lax.rem(x + nx - d, nx) for d in range(nx)]
     t_at = [lax.rem(tp + d, ntp) for d in range(ntp)]
-
+    fetch = pltpu.make_async_copy(w_hbm, w_ref, wsem)
+    fetch.start()
+    local = [
+        pltpu.make_async_copy(
+            g_ref.at[:, pl.ds(f * depth, depth)], held.at[z, x, f], csem.at[f]
+        )
+        for f in range(halves)
+    ]
+    for f in range(halves):
+        local[f].start()
+
+    up, down = z < nz - 1, z > 0
     barrier = pltpu.get_barrier_semaphore()
     for d in range(1, nx):
         pl.semaphore_signal(barrier, inc=1, device_id=(z * nx + x_at[d], tp), device_id_type=MESH)
-    for d in range(1, nz):
-        pl.semaphore_signal(barrier, inc=1, device_id=(z_at[d] * nx + x, tp), device_id_type=MESH)
     for d in range(1, ntp):
         pl.semaphore_signal(barrier, inc=1, device_id=(kv, t_at[d]), device_id_type=MESH)
-    local = pltpu.make_async_copy(g_ref, held.at[z, x], csem)
-    local.start()
-    pl.semaphore_wait(barrier, nx - 1 + nz - 1 + ntp - 1)
-
-    def along_z(d):
-        return remote(g_ref, held.at[z, x], zss.at[d], zrs.at[d], (z_at[d] * nx + x, tp))
-
-    def landed_z(k):
-        return remote(g_ref, held.at[z_from[k], x], zss.at[k], zrs.at[k],
-                      (z_at[k] * nx + x, tp))
-
-    def along_x(k, d):
-        return remote(held.at[z_from[k], x], held.at[z_from[k], x],
-                      xss.at[k, d], xrs.at[k, d], (z * nx + x_at[d], tp))
-
-    def landed_x(k, d):
-        return remote(held.at[z_from[k], x], held.at[z_from[k], x_from[d]],
-                      xss.at[k, d], xrs.at[k, d], (z * nx + x_at[d], tp))
-
-    def own_x(d):
-        return remote(g_ref, held.at[z, x], xss.at[0, d], xrs.at[0, d],
-                      (z * nx + x_at[d], tp))
-
     for d in range(1, nz):
-        along_z(d).start()
-    for d in range(1, nx):
-        own_x(d).start()
-    local.wait()
-    for k in range(nz):
-        if k > 0:
-            landed_z(k).wait_recv()
+        pl.semaphore_signal(
+            barrier, inc=1, device_id=(lax.rem(z + d, nz) * nx + x, tp), device_id_type=MESH
+        )
+    pl.semaphore_wait(barrier, nx - 1 + ntp - 1 + nz - 1)
+
+    def along_z(origin, f, step):
+        return remote(held.at[origin, x, f], held.at[origin, x, f], zss.at[origin, f, (step + 1) // 2],
+                      zrs.at[origin, f], (kv + step * nx, tp))
+
+    def along_x(origin, f, d):
+        return remote(held.at[origin, x, f], held.at[origin, x, f], xss.at[origin, f, d],
+                      xrs.at[origin, f, d], (z * nx + x_at[d], tp))
+
+    def landed_x(origin, f, d):
+        source = lax.rem(x + nx - d, nx)
+        return remote(held.at[origin, x, f], held.at[origin, source, f], xss.at[origin, f, d],
+                      xrs.at[origin, f, d], (z * nx + x_at[d], tp))
+
+    for f in range(halves):
+        local[f].wait()
+        for side, step in ((up, 1), (down, -1)):
+            @pl.when(side)
+            def _():
+                along_z(z, f, step).start()
+        for d in range(1, nx):
+            along_x(z, f, d).start()
+
+    def multiply(origin):
+        product = jnp.zeros((nx * rows, w_ref.shape[1]), jnp.float32)
+        for f in range(halves):
             for d in range(1, nx):
-                along_x(k, d).start()
-
-    def to_tp(block, j):
-        target = block * pieces + j
-        return target
-
-    for k in range(nz):
-        for d in range(1, nx):
-            landed_x(k, d).wait_recv()
-        block = z_from[k]
-        product = jnp.dot(
-            held[block].reshape(nx * rows, held.shape[3]), w_ref[...],
-            preferred_element_type=jnp.float32,
-        )
+                landed_x(origin, f, d).wait_recv()
+            product = product + jnp.dot(
+                held[origin, :, f].reshape(nx * rows, depth), w_ref[f * depth:(f + 1) * depth],
+                preferred_element_type=jnp.float32,
+            )
         for j in range(pieces):
-            parts[block * pieces + j] = product[j * per:(j + 1) * per].astype(jnp.bfloat16)
-            target = block * pieces + j
+            target = origin * pieces + j
+            parts[target] = product[j * per:(j + 1) * per].astype(jnp.bfloat16)
 
             @pl.when(target != tp)
             def _():
                 remote(parts.at[target], got.at[tp], tss.at[target], trs.at[tp],
                        (kv, target)).start()
+
+    def relay(k):
+        for f in range(halves):
+            for step in (1, -1):
+                origin = z - step * k
+
+                @pl.when((origin >= 0) & (origin < nz))
+                def _():
+                    along_z(origin, f, step).wait_recv()
+                    follow = up if step == 1 else down
+
+                    @pl.when(follow)
+                    def _():
+                        along_z(origin, f, step).start()
+
+                    for d in range(1, nx):
+                        along_x(origin, f, d).start()
+
+    for k in range(1, nz):
+        relay(k)
+        if k == 1:
+            fetch.wait()
+            multiply(z)
+        for step in (1, -1):
+            near = z - step * (k - 1)
+            if k > 1:
+                @pl.when((near >= 0) & (near < nz))
+                def _():
+                    multiply(near)
+    if nz == 1:
+        fetch.wait()
+        multiply(z)
+    else:
+        for step in (1, -1):
+            last = z - step * (nz - 1)
+
+            @pl.when((last >= 0) & (last < nz))
+            def _():
+                multiply(last)
 
     summed = parts[tp].astype(jnp.float32)
     for d in range(1, ntp):
@@ -415,31 +463,39 @@
                (kv, source)).wait()
         summed = summed + got[source].astype(jnp.float32)
     out_ref[...] = summed.astype(out_ref.dtype)
-    for d in range(1, nz):
-        along_z(d).wait_send()
-    for d in range(1, nx):
-        own_x(d).wait_send()
-        for k in range(1, nz):
-            along_x(k, d).wait_send()
+    for f in range(halves):
+        for origin in range(nz):
+            for d in range(1, nx):
+                along_x(origin, f, d).wait_send()
+
+            @pl.when(up & (origin <= z))
+            def _():
+                along_z(origin, f, 1).wait_send()
+
+            @pl.when(down & (origin >= z))
+            def _():
+                along_z(origin, f, -1).wait_send()
 
 
 def output(nx, nz, ntp, gated, w_out):
     rows, depth = gated.shape
     columns = w_out.shape[1]
+    halves = 2
     per = rows * nx * nz // ntp
     bf, dma = jnp.bfloat16, pltpu.SemaphoreType.DMA
     vmem = pl.BlockSpec(memory_space=pltpu.VMEM)
     return pl.pallas_call(
         functools.partial(output_kernel, nx, nz, ntp),
         out_shape=jax.ShapeDtypeStruct((per, columns), bf),
-        in_specs=[vmem, vmem],
+        in_specs=[vmem, pl.BlockSpec(memory_space=pl.ANY)],
         out_specs=vmem,
         scratch_shapes=[
-            pltpu.VMEM((nz, nx, rows, depth), bf),
+            pltpu.VMEM((nz, nx, halves, rows, depth // halves), bf),
             pltpu.VMEM((ntp, per, columns), bf),
             pltpu.VMEM((ntp, per, columns), bf),
-            dma((nz,)), dma((nz,)), dma((nz, nx)), dma((nz, nx)),
-            dma((ntp,)), dma((ntp,)), dma(()),
+            pltpu.VMEM(w_out.shape, bf),
+            dma((nz, halves, 2)), dma((nz, halves)), dma((nz, halves, nx)), dma((nz, halves, nx)),
+            dma((ntp,)), dma((ntp,)), dma((halves,)), dma(()),
         ],
         compiler_params=pltpu.CompilerParams(
             collective_id=1, has_side_effects=True, vmem_limit_bytes=VMEM_LIMIT
@@ -452,35 +508,21 @@
     decay_rate, head_gain, carried_state, last_keys, last_values, last_writes, last_decays,
     accepted,
 ):
-    f32 = jnp.float32
     nz = 4 if nkv % 4 == 0 else 1
     nx = nkv // nz
     local_width = hidden.shape[1]
-    seqs, heads = carried_state.shape[:2]
-    steps = last_keys.shape[1]
-    rows = seqs * steps
-    wide = hidden.astype(f32)
-    local_sq = jnp.sum(wide * wide, -1, keepdims=True)
+    heads = carried_state.shape[1]
     gain = lax.dynamic_slice_in_dim(norm_gain, lax.axis_index("kv") * local_width, local_width)
-    scaled = (wide * gain.astype(f32)).astype(jnp.bfloat16)
-    w_small = jnp.concatenate([w_write, w_decay], 1)
-    small = jnp.dot(scaled, w_small, preferred_element_type=f32)
-    fill = LANES - 2 * heads - 1
-    small = jnp.concatenate(
-        [small, local_sq, jnp.zeros((small.shape[0], fill), f32)], 1
-    ).astype(jnp.bfloat16)
+    w_small = jnp.concatenate(
+        [w_write, w_decay, jnp.zeros((local_width, LANES - 2 * heads), w_write.dtype)], 1
+    )
     plan, (projected, small) = project(
-        nx, nz, scaled, small, (w_query, w_key, w_value, w_gate), 2 * heads, local_width * nkv
+        nx, nz, hidden, gain[None, :], w_small, (w_query, w_key, w_value, w_gate),
+        2 * heads, local_width * nkv,
     )
-    taken = (jnp.arange(steps, dtype=jnp.int32)[None, :] < accepted[:, None]).astype(f32)
-    last_small = jnp.concatenate(
-        [last_writes.reshape(rows, heads), last_decays.reshape(rows, heads),
-         taken.reshape(rows, 1), jnp.zeros((rows, fill), f32)], 1
-    )
-    rates = jnp.pad(decay_rate, (0, LANES - heads))[None, :]
     gated, committed = core(
-        plan, projected, small, last_keys, last_values, last_small, rates,
-        head_gain[None, :], carried_state,
+        plan, projected, small, last_keys, last_values, last_writes, last_decays,
+        accepted[:, None], decay_rate[None, :], head_gain[None, :], carried_state,
     )
     return (output(nx, nz, ntp, gated, w_out), committed)
 

time: 171 us -> 159 us (0.930); the launches traced: 167 us -> 158 us
  Pallas kernels: 153 us -> 148 us
  other arithmetic: 4.22 us -> 0.77 us
    pallas_call x1, Pallas kernels: 38.8 us -> 31.3 us  [output(): pl.pallas_call(functools.partial(output_kernel, nx, nz, ntp), out_shape=j...]
    reshape x3 -> x0, local copies, waits for them, and re-layouts: 4.16 us -> none  [the longest x1 1.7 us: core(): last_values.reshape(rows, heads * dv)]
    unnamed x7 -> x5, local copies, waits for them, and re-layouts: 3.17 us -> 6.06 us
    pallas_call x1, Pallas kernels: 28.9 us -> 31.3 us  [core(): pl.pallas_call(functools.partial(core_kernel, heads), grid=(heads,), out_...]
where the time goes in v2:
time: 159 us; the launch traced here: 158 us
  Pallas kernels  148 us (93%)
  local copies, waits for them, and re-layouts  8.81 us (6%)
    pallas_call x1, Pallas kernels, project(): pl.pallas_call(functools.partial(project_kernel, nx, nz, plan, width, sq_...  85.2 us
    pallas_call x1, Pallas kernels, output(): pl.pallas_call(functools.partial(output_kernel, nx, nz, ntp), out_shape=j...  31.3 us
    pallas_call x1, Pallas kernels, core(): pl.pallas_call(functools.partial(core_kernel, heads), grid=(heads,), out_...  31.3 us
    unnamed x5, local copies, waits for them, and re-layouts  6.06 us

profile of v2, /device:TPU:0, one launch (start us, length us, event | category | flops | bytes accessed | tf_op | source)
XLA Modules:
  0.0 158.0 jit_solution(7389459750310816507)
XLA Ops:
  0.6 0.8 dynamic_slice.3
  1.4 0.1 pad.2.clone
  1.5 0.6 broadcast_in_dim.15.n_ref
  2.1 1.3 copy.23.acc_ref
  3.4 1.4 copy.21.lw_ref
  4.8 1.4 copy.22.ld_ref
  6.2 0.9 copy.19
  7.0 0.9 copy.20
  7.9 0.8 maximum_maximum_fusion.ws_ref
  8.7 85.2 %shard_map.176 = (f32[12,64,512]{2,1,0:T(8,128)}, f32[64,128]{1,0:T(8,128)}) custom-call(bf16[512,512]{1,0:T(8,128)(2,1)} %h_ref.1, bf16[1,512]{1,0:T(2,128)(2,1)} %broadcast_in_dim.15.n_ref, bf16[512,128]{1,0:T(8,128)(2,1)} %maximum_maximum_fusion.ws_ref, bf16[512,1024]{1,0:T(8,128)(2,1)} %wq.1, bf16[512,1024]{1,0:T(8,128)(2,1)} %wk.1, ...), custom_call_target="tpu_custom_call" | custom-call | tf_op jit(solution)/shard_map/pallas_call | solution.py:142
  93.8 31.3 %shard_map.177 = (bf16[64,2048]{1,0:T(8,128)(2,1)}, f32[16,8,128,256]{3,2,1,0:T(8,128)}) custom-call(f32[12,64,512]{2,1,0:T(8,128)} %get-tuple-element.6.q_ref.k_ref.v_ref.g_ref, f32[12,64,512]{2,1,0:T(8,128)} %get-tuple-element.6.q_ref.k_ref.v_ref.g_ref, f32[12,64,512]{2,1,0:T(8,128)} %get-tuple-element.6.q_ref.k_ref.v_ref.g_ref, ...), custom_call_target="tpu_custom_call" | custom-call | tf_op jit(solution)/shard_map/pallas_call | solution.py:312
  125.1 31.3 %shard_map.178 = bf16[128,512]{1,0:T(8,128)(2,1)} custom-call(bf16[64,2048]{1,0:T(8,128)(2,1)} %get-tuple-element.8.g_ref, bf16[2048,512]{1,0:T(8,128)(2,1)} %w_hbm.1), custom_call_target="tpu_custom_call" | custom-call | tf_op jit(solution)/shard_map/pallas_call | solution.py:487
  156.5 1.6 copy.25
  (1 shorter events, 0.0 us)

commit v3 on v2

--- a/solution.py
+++ b/solution.py
@@ -198,14 +198,14 @@
 
 
 def core_kernel(
-    heads, q_ref, k_ref, v_ref, g_ref, small_ref, lk_ref, lv_ref, lw_ref, ld_ref, acc_ref, rate_ref,
+    heads, q_ref, k_ref, v_ref, g_ref, small_ref, lk_ref, lv_ref, lsmall_ref, rate_ref,
     gain_ref, state_ref, gated_ref, com_ref, left, prod, kd, fr, dec, old_k, old_v, wide_v, gout,
 ):
     h = pl.program_id(0)
     seqs = state_ref.shape[0]
     steps = q_ref.shape[1] // seqs
     dk, dv = q_ref.shape[2], v_ref.shape[2]
-    pad = left.shape[1]
+    pad = kd.shape[1]
     bf, f32 = jnp.bfloat16, jnp.float32
 
     def at_t(ref, t):
@@ -232,25 +232,23 @@
 
     old_k[...] = lk_ref[...].astype(f32)
     old_v[...] = lv_ref[...].astype(f32)
-    taken = [(acc_ref[...] > t).astype(f32) for t in every]
-    write = [jax.nn.sigmoid(column(lw_ref[:, t, :], h)) * taken[t] for t in every]
-    decay = [-rate * jax.nn.softplus(column(ld_ref[:, t, :], h)) * taken[t] for t in every]
+    old = [at_t(lsmall_ref, t) for t in every]
+    taken = [column(m, 2 * heads) for m in old]
+    write = [jax.nn.sigmoid(column(old[t], h)) * taken[t] for t in every]
+    decay = [-rate * jax.nn.softplus(column(old[t], heads + h)) * taken[t] for t in every]
     keys = [unit(old_k[:, t, :]) for t in every]
-    running, u_val, u_key = solve(keys, [old_v[:, t, :] for t in every], write, decay)
+    running, old_val, u_key = solve(keys, [old_v[:, t, :] for t in every], write, decay)
+    faded = [keys[t] * jnp.exp(running[-1] - running[t]) for t in every]
+    kept = jnp.exp(running[-1])
     for t in every:
         left[:, t, :] = u_key[t]
-        kd[:, t, :] = keys[t] * jnp.exp(running[-1] - running[t])
-    dec[...] = jnp.broadcast_to(jnp.exp(running[-1]), (seqs, dv))
+        kd[:, t, :] = faded[t]
+    dec[...] = jnp.broadcast_to(kept, (seqs, dv))
     for t in range(steps, pad):
-        left[:, t, :] = jnp.zeros((seqs, dk), f32)
         kd[:, t, :] = jnp.zeros((seqs, dk), f32)
         fr[:, t, :] = jnp.zeros((seqs, dv), f32)
-    for b in range(seqs):
-        prod[b] = jnp.dot(
-            left[b].astype(bf), state_ref[b, 0].astype(bf), preferred_element_type=f32
-        )
-    for t in every:
-        fr[:, t, :] = u_val[t] - prod[:, t, :]
+    for t in range(3 * steps, left.shape[1]):
+        left[:, t, :] = jnp.zeros((seqs, dk), f32)
 
     small = [at_t(small_ref, t) for t in every]
     write = [jax.nn.sigmoid(column(small[t], h)) for t in every]
@@ -260,22 +258,34 @@
         wide_v[j] = silu(v_ref[0, :, cut(j)])
     keys = [unit(silu(at_t(k_ref.at[0], t))) for t in every]
     running, u_val, u_key = solve(keys, [value_at(wide_v, t) for t in every], write, decay)
+    rotated = [queries[t] * jnp.exp(running[t]) for t in every]
     for t in every:
-        left[:, t, :] = u_key[t]
-        left[:, steps + t, :] = queries[t] * jnp.exp(running[t])
+        left[:, steps + t, :] = u_key[t]
+        left[:, 2 * steps + t, :] = rotated[t]
+    for b in range(seqs):
+        prod[b] = jnp.dot(
+            left[b].astype(bf), state_ref[b, 0].astype(bf), preferred_element_type=f32
+        )
+    old_fresh = [old_val[t] - prod[:, t, :] for t in every]
+    for t in every:
+        fr[:, t, :] = old_fresh[t]
     for b in range(seqs):
         added = lax.dot_general(
             kd[b].astype(bf), fr[b].astype(bf), (((0,), (0,)), ((), ())),
             preferred_element_type=f32,
         )
-        after = state_ref[b, 0] * dec[b:b + 1, :] + added
-        com_ref[b, 0] = after
-        prod[b] = jnp.dot(left[b].astype(bf), after.astype(bf), preferred_element_type=f32)
+        com_ref[b, 0] = state_ref[b, 0] * dec[b:b + 1, :] + added
+
+    def through(rows, at):
+        total = kept * prod[:, at, :]
+        for s in every:
+            total = total + jnp.sum(rows * faded[s], -1, keepdims=True) * old_fresh[s]
+        return total
 
     gain = gain_ref[...]
-    fresh = [u_val[t] - prod[:, t, :] for t in every]
+    fresh = [u_val[t] - through(u_key[t], steps + t) for t in every]
     for t in every:
-        result = prod[:, steps + t, :]
+        result = through(rotated[t], 2 * steps + t)
         for s in range(t + 1):
             score = jnp.sum(queries[t] * keys[s], -1, keepdims=True)
             score = score * jnp.exp(running[t] - running[s])
@@ -288,8 +298,7 @@
         gated_ref[:, cut(j)] = (gout[j] * silu(g_ref[0, :, cut(j)])).astype(bf)
 
 
-def core(plan, projected, small, last_keys, last_values, last_writes, last_decays, accepted,
-         rates, head_gain, state):
+def core(plan, projected, small, last_keys, last_values, last_small, rates, head_gain, state):
     seqs, heads, dk, dv = state.shape
     steps = last_keys.shape[1]
     rows = seqs * steps
@@ -321,13 +330,12 @@
             whole((rows, LANES)),
             pl.BlockSpec((seqs, steps, dk), lambda h: (0, 0, h)),
             pl.BlockSpec((seqs, steps, dv), lambda h: (0, 0, h)),
-            whole((seqs, steps, heads)), whole((seqs, steps, heads)), whole((seqs, 1)),
-            whole((1, heads)), whole((1, dv)), state_block,
+            whole((rows, LANES)), whole((1, heads)), whole((1, dv)), state_block,
         ],
         out_specs=(pl.BlockSpec((rows, dv), lambda h: (0, h)), state_block),
         scratch_shapes=[
-            pltpu.VMEM((seqs, pad, dk), f32),
-            pltpu.VMEM((seqs, pad, dv), f32),
+            pltpu.VMEM((seqs, 2 * pad, dk), f32),
+            pltpu.VMEM((seqs, 2 * pad, dv), f32),
             pltpu.VMEM((seqs, pad, dk), f32),
             pltpu.VMEM((seqs, pad, dv), f32),
             pltpu.VMEM((seqs, dv), f32),
@@ -339,7 +347,7 @@
         compiler_params=pltpu.CompilerParams(vmem_limit_bytes=VMEM_LIMIT),
     )(
         projected, projected, projected, projected, small,
-        last_keys, last_values, last_writes, last_decays, accepted, rates, head_gain, state,
+        last_keys, last_values, last_small, rates, head_gain, state,
     )
 
 
@@ -520,9 +528,16 @@
         nx, nz, hidden, gain[None, :], w_small, (w_query, w_key, w_value, w_gate),
         2 * heads, local_width * nkv,
     )
+    seqs, steps = last_keys.shape[:2]
+    rows = seqs * steps
+    taken = (jnp.arange(steps, dtype=jnp.int32)[None, :] < accepted[:, None]).astype(jnp.float32)
+    last_small = jnp.concatenate(
+        [last_writes.reshape(rows, heads), last_decays.reshape(rows, heads),
+         taken.reshape(rows, 1), jnp.zeros((rows, LANES - 2 * heads - 1), jnp.float32)], 1
+    )
     gated, committed = core(
-        plan, projected, small, last_keys, last_values, last_writes, last_decays,
-        accepted[:, None], decay_rate[None, :], head_gain[None, :], carried_state,
+        plan, projected, small, last_keys, last_values, last_small, decay_rate[None, :],
+        head_gain[None, :], carried_state,
     )
     return (output(nx, nz, ntp, gated, w_out), committed)
 

time: 159 us -> 144 us (0.906)
  Pallas kernels: 148 us -> 135 us
  local copies, waits for them, and re-layouts: 8.81 us -> 6.45 us
    pallas_call x1, Pallas kernels: 31.3 us -> 18.1 us  [core(): pl.pallas_call(functools.partial(core_kernel, heads), grid=(heads,), out_...]
where the time goes in v3:
time: 144 us
  Pallas kernels  135 us (94%)
  local copies, waits for them, and re-layouts  6.45 us (4%)
  other arithmetic  2.19 us (2%)
    pallas_call x1, Pallas kernels, project(): pl.pallas_call(functools.partial(project_kernel, nx, nz, plan, width, sq_...  85.2 us
    pallas_call x1, Pallas kernels, output(): pl.pallas_call(functools.partial(output_kernel, nx, nz, ntp), out_shape=j...  31.3 us
    pallas_call x1, Pallas kernels, core(): pl.pallas_call(functools.partial(core_kernel, heads), grid=(heads,), out_...  18.1 us
    unnamed x5, local copies, waits for them, and re-layouts  4.87 us

profile of v3, /device:TPU:0, one launch (start us, length us, event | category | flops | bytes accessed | tf_op | source)
XLA Modules:
  0.0 143.9 jit_solution(14194979244472351189)
XLA Ops:
  0.6 0.8 dynamic_slice.3
  1.4 0.1 pad.6.clone
  1.5 0.1 pad.3.clone
  1.6 0.6 broadcast_in_dim.17.n_ref
  2.1 0.7 fusion
  2.9 0.1 reshape.42
  2.9 0.8 copy.26
  3.7 0.8 copy.27
  4.5 0.7 maximum_maximum_fusion.1.lsmall_ref
  5.2 0.9 copy.24
  6.1 0.9 copy.25
  6.9 0.8 maximum_maximum_fusion.ws_ref
  7.7 85.2 %shard_map.176 = (f32[12,64,512]{2,1,0:T(8,128)}, f32[64,128]{1,0:T(8,128)}) custom-call(bf16[512,512]{1,0:T(8,128)(2,1)} %h_ref.1, bf16[1,512]{1,0:T(2,128)(2,1)} %broadcast_in_dim.17.n_ref, bf16[512,128]{1,0:T(8,128)(2,1)} %maximum_maximum_fusion.ws_ref, bf16[512,1024]{1,0:T(8,128)(2,1)} %wq.1, bf16[512,1024]{1,0:T(8,128)(2,1)} %wk.1, ...), custom_call_target="tpu_custom_call" | custom-call | tf_op jit(solution)/shard_map/pallas_call | solution.py:142
  92.9 18.1 %shard_map.177 = (bf16[64,2048]{1,0:T(8,128)(2,1)}, f32[16,8,128,256]{3,2,1,0:T(8,128)}) custom-call(f32[12,64,512]{2,1,0:T(8,128)} %get-tuple-element.6.q_ref.k_ref.v_ref.g_ref, f32[12,64,512]{2,1,0:T(8,128)} %get-tuple-element.6.q_ref.k_ref.v_ref.g_ref, f32[12,64,512]{2,1,0:T(8,128)} %get-tuple-element.6.q_ref.k_ref.v_ref.g_ref, ...), custom_call_target="tpu_custom_call" | custom-call | tf_op jit(solution)/shard_map/pallas_call | solution.py:321
  111.0 31.3 %shard_map.178 = bf16[128,512]{1,0:T(8,128)(2,1)} custom-call(bf16[64,2048]{1,0:T(8,128)(2,1)} %get-tuple-element.8.g_ref, bf16[2048,512]{1,0:T(8,128)(2,1)} %w_hbm.1), custom_call_target="tpu_custom_call" | custom-call | tf_op jit(solution)/shard_map/pallas_call | solution.py:495
  142.3 1.6 %copy.30 = bf16[128,512]{1,0:T(8,128)(2,1)} copy(bf16[128,512]{1,0:T(8,128)(2,1)} %shard_map.178) | data formatting | bytes 262144
  (2 shorter events, 0.0 us)
